TPU v7x, 32 devices: a whole 2x2x4 slice. The times are simulated.
32 devices in a mesh: ep: 8 (over z, x), tp: 4 (over y, core).
Axes of the slice: x: 2, y: 2, z: 4, core: 2. Of those that a mesh axis runs over, the one named last changes fastest.
Arguments:
- mixer_rows: bfloat16 [1024, 2048], P('ep'), may hold values from -40 to 40
- mixer_gain: float32 [2048], replicated, may hold values from 0.1 to 1.9
- inner_weight: bfloat16 [2048, 1024], P(None, 'tp'), may hold values from -0.125 to 0.125
- gate_in_weight: bfloat16 [2048, 1024], P(None, 'tp'), may hold values from -0.125 to 0.125
- gate_out_weight: bfloat16 [2048, 1024], P(None, 'tp'), may hold values from -0.125 to 0.125
- conv_taps: float32 [3, 1024], P(None, 'tp'), may hold values from -3.5 to 3.5
- mixer_out_weight: bfloat16 [1024, 2048], P('tp'), may hold values from -0.1875 to 0.1875
- routed_rows: bfloat16 [2048, 2048], P('ep'), may hold values from -40 to 40
- routed_gain: float32 [2048], replicated, may hold values from 0.1 to 1.9
- route_ids: int32 [2048, 2], P('ep'), may hold values from 0 to 7, all different within a row; in each aligned block of 256 rows (0 to 255, 256 to 511, ...) at most 128 rows name the same one
- route_weights: float32 [2048, 2], P('ep'), may hold values from 0.25 to 1
- expert_gate: bfloat16 [8, 2048, 2048], P('ep', None, 'tp'), may hold values from -0.125 to 0.125
- expert_up: bfloat16 [8, 2048, 2048], P('ep', None, 'tp'), may hold values from -0.125 to 0.125
- expert_down: bfloat16 [8, 2048, 2048], P('ep', 'tp'), may hold values from -0.125 to 0.125
Outputs:
- mixer_output: bfloat16 [1024, 2048], P('ep')
- routed_output: bfloat16 [2048, 2048], P('ep')
Inputs may be any that keep to these rules, and one draw needn't show every extreme that they name: `route_ids`: within each aligned block of 256 tokens, no expert is named by more than 128 choices, a bound that some block reaches; a token's 2 experts differ.
All inputs are finite; a program needn't handle non-finite values.
Results may differ from a plain program's by a relative error of at most 0.019.
Values may be sent and summed in bfloat16 or wider, within the bound.
A program may use at most 64 MiB of HBM per device.

v0:
```python
import jax
import jax.numpy as jnp
from jax import lax
from jax.sharding import PartitionSpec as P


def shifted(value, axis, steps):
    count = lax.axis_size(axis)
    initial, last = (max(0, -steps), min(count, count - steps))
    return lax.ppermute(value, axis, [(source, source + steps) for source in range(initial, last)])


def rms_scale(row_block, gain_row):
    values = row_block.astype(jnp.float32)
    scaled = values * lax.rsqrt(jnp.mean(values * values, axis=-1, keepdims=True) + 1e-06)
    return (scaled * gain_row).astype(jnp.bfloat16)


def on_device(
    mixer_rows,
    mixer_gain,
    inner_weight,
    gate_in_weight,
    gate_out_weight,
    conv_taps,
    mixer_out_weight,
    routed_rows,
    routed_gain,
    route_ids,
    route_weights,
    expert_gate,
    expert_up,
    expert_down,
):
    normed = rms_scale(mixer_rows, mixer_gain)
    inner_proj = jnp.dot(normed, inner_weight, preferred_element_type=jnp.float32)
    gate_in = jnp.dot(normed, gate_in_weight, preferred_element_type=jnp.float32)
    conv_input = (gate_in * inner_proj).astype(jnp.bfloat16)
    gate_out = jnp.dot(normed, gate_out_weight, preferred_element_type=jnp.float32)
    tap_total = conv_taps.shape[0]
    rim_rows = tap_total - 1
    earlier_rows = shifted(conv_input[conv_input.shape[0] - rim_rows :], "ep", 1)
    extended = jnp.concatenate([earlier_rows, conv_input], axis=0).astype(jnp.float32)
    length = conv_input.shape[0]
    conv_out = jnp.zeros(conv_input.shape, jnp.float32)
    for tap_index in range(tap_total):
        conv_out = conv_out + conv_taps[tap_index] * extended[tap_index : tap_index + length]
    gated_conv = (gate_out * conv_out).astype(jnp.bfloat16)
    mixer_terms = jnp.dot(gated_conv, mixer_out_weight, preferred_element_type=jnp.float32)
    routed_normed = rms_scale(routed_rows, routed_gain)
    experts = lax.axis_size("ep")
    groups = lax.axis_size("tp")
    column = lax.axis_index("tp")
    tok_count, pick_count = route_ids.shape
    model_width = routed_rows.shape[1]
    capacity = 2 * tok_count * pick_count // experts
    share_rows = capacity // groups
    flat_ids = route_ids.reshape(-1)
    onehot = (flat_ids[:, None] == jnp.arange(experts, dtype=jnp.int32)[None, :]).astype(jnp.int32)
    slot_rank = jnp.sum((jnp.cumsum(onehot, axis=0) - onehot) * onehot, axis=1)
    slot_number = slot_rank * experts + flat_ids
    owners = jnp.arange(tok_count * pick_count, dtype=jnp.int32) // pick_count
    matches = slot_number[None, :] == jnp.arange(capacity * experts, dtype=jnp.int32)[:, None]
    token_table = jnp.where(
        jnp.any(matches, axis=1), jnp.sum(jnp.where(matches, owners[None, :], 0), axis=1), tok_count
    )
    padded_rows = jnp.concatenate(
        [routed_normed, jnp.zeros((1, model_width), jnp.bfloat16)], axis=0
    )
    table_share = lax.dynamic_slice_in_dim(
        token_table.reshape(capacity, experts), column * share_rows, share_rows, 0
    )
    outgoing = jnp.take(padded_rows, table_share.reshape(-1), axis=0).reshape(
        share_rows, experts, model_width
    )
    arrived = lax.all_to_all(outgoing, "ep", split_axis=1, concat_axis=1, tiled=True)
    incoming = lax.all_gather(arrived, "tp", axis=0, tiled=True)
    slot_rows = incoming.reshape(capacity * experts, model_width)
    gate_act = jnp.dot(slot_rows, expert_gate[0], preferred_element_type=jnp.float32)
    up_act = jnp.dot(slot_rows, expert_up[0], preferred_element_type=jnp.float32)
    hidden = (jax.nn.silu(gate_act) * up_act).astype(jnp.bfloat16)
    summed = lax.psum_scatter(
        jnp.dot(hidden, expert_down[0], preferred_element_type=jnp.float32).astype(jnp.bfloat16),
        "tp",
        scatter_dimension=0,
        tiled=True,
    )
    returned = lax.all_to_all(
        summed.reshape(share_rows, experts, model_width),
        "ep",
        split_axis=1,
        concat_axis=1,
        tiled=True,
    )
    flat_back = jnp.concatenate(
        [
            returned.reshape(share_rows * experts, model_width),
            jnp.zeros((1, model_width), jnp.bfloat16),
        ],
        axis=0,
    )
    local_slot = jnp.where(
        slot_rank // share_rows == column,
        (slot_rank - column * share_rows) * experts + flat_ids,
        share_rows * experts,
    )
    contrib = (
        jnp.take(flat_back, local_slot, axis=0).astype(jnp.float32)
        * route_weights.reshape(-1)[:, None]
    )
    routed_terms = jnp.sum(contrib.reshape(tok_count, pick_count, model_width), axis=1)
    mixer_total, routed_total = (
        lax.psum(mixer_terms.astype(jnp.bfloat16), "tp").astype(jnp.float32),
        lax.psum(routed_terms.astype(jnp.bfloat16), "tp").astype(jnp.float32),
    )
    return (mixer_total.astype(jnp.bfloat16), routed_total.astype(jnp.bfloat16))


def solution(mesh):
    return jax.shard_map(
        on_device,
        mesh=mesh,
        in_specs=(
            P("ep", None),
            P(),
            P(None, "tp"),
            P(None, "tp"),
            P(None, "tp"),
            P(None, "tp"),
            P("tp", None),
            P("ep", None),
            P(),
            P("ep", None),
            P("ep", None),
            P("ep", None, "tp"),
            P("ep", None, "tp"),
            P("ep", "tp", None),
        ),
        out_specs=(P("ep", None), P("ep", None)),
        check_vma=False,
    )
```

profile of v0, /device:TPU:0, one launch (start us, length us, event | category | flops | bytes accessed | tf_op | source)
XLA Modules:
  0.0 255.2 jit_solution(8111063935972421025)
XLA Ops:
  8.5 1.1 reduce-window.6
  10.9 1.5 fusion.4
  13.6 2.3 gather_fusion
  15.9 2.4 copy_select_fusion
  18.4 32.8 %all_to_all.10 = bf16[32,8,2048]{2,0,1:T(8,128)(2,1)S(1)} all-to-all(bf16[32,8,2048]{2,0,1:T(8,128)(2,1)S(1)} %copy_select_fusion), channel_id=1, replica_groups=mesh['ep'=8,'tp'=4] {'ep'}, dimensions={1} | all-to-all | bytes 2097152 | tf_op jit(solution)/shard_map/all_to_all | solution.py:76
  51.2 1.5 copy.77
  52.8 33.6 %all-gather.2.cloned.1.call-done = bf16[128,8,2048]{2,1,0:T(8,128)(2,1)} async-done(((bf16[32,8,2048]{2,1,0:T(8,128)(2,1)}), bf16[128,8,2048]{2,1,0:T(8,128)(2,1)}) %all-gather.2.cloned.1.call-update) | async-done | bytes 4194320 | tf_op jit(solution)/shard_map/all_gather | solution.py:77
  86.4 6.6 %fusion.2 = f32[1024,512]{1,0:T(8,128)} fusion(bf16[128,8,2048]{2,1,0:T(8,128)(2,1)} %all-gather.2.cloned.1.call-done, bf16[1,2048,512]{2,1,0:T(8,128)(2,1)} %param.25), kind=kOutput, calls=%fused_computation.4 | convolution fusion | flops 2147483648 | bytes 8388608 | tf_op jit(solution)/shard_map/dot_general | solution.py:79
  93.0 10.0 %convolution_convert_fusion = bf16[1024,2048]{1,0:T(8,128)(2,1)} fusion(bf16[1,512,2048]{2,1,0:T(8,128)(2,1)S(1)} %copy-done, f32[1024,512]{1,0:T(8,128)} %fusion.2, bf16[1,2048,512]{2,1,0:T(8,128)(2,1)} %param.26, bf16[128,8,2048]{2,1,0:T(8,128)(2,1)} %all-gather.2.cloned.1.call-done), kind=kOutput, calls=%fused_computation.8 | convolution fusion | flops 4300210176 | bytes 14680064 | tf_op jit(solution)/shard_map/dot_general | solution.py:83
  103.0 1.0 copy-done.2
  104.2 43.5 %reduce-scatter.2.cloned.1.call-done = bf16[256,2048]{1,0:T(8,128)(2,1)} async-done(((bf16[1024,2048]{1,0:T(8,128)(2,1)}), bf16[256,2048]{1,0:T(8,128)(2,1)}) %reduce-scatter.2.cloned.1.call-update) | async-done | bytes 1048592 | tf_op jit(solution)/shard_map/reduce_scatter | solution.py:82
  147.7 2.8 %copy.78 = bf16[32,8,2048]{2,0,1:T(8,128)(2,1)} copy(bf16[32,8,2048]{2,1,0:T(8,128)(2,1)} %bitcast.47) | data formatting | bytes 2097152 | tf_op jit(solution)/shard_map/reshape | solution.py:89
  150.5 5.5 %all-to-all-start.1 = ((bf16[32,8,2048]{2,0,1:T(8,128)(2,1)}), bf16[32,8,2048]{2,0,1:T(8,128)(2,1)S(1)}, u32[]{:S(2)}, u32[]{:S(2)}) async-start(bf16[32,8,2048]{2,0,1:T(8,128)(2,1)} %copy.78), calls=%async_computation.2 | async-start | bytes 2097152 | tf_op jit(solution)/shard_map/all_to_all | solution.py:88
  156.1 1.7 fusion.40
  157.9 1.8 fusion.16
  159.7 4.1 %collective-permute-start = (bf16[2,256]{1,0:T(2,128)(2,1)S(1)}, bf16[2,256]{1,0:T(2,128)(2,1)S(1)}, u32[]{:S(2)}, u32[]{:S(2)}) collective-permute-start(bf16[2,256]{1,0:T(2,128)(2,1)S(1)} %slice.40), channel_id=1, source_target_pairs={{0,4},{4,8},{8,12},{12,16},{16,20},{20,24},{24,28},{1,5},{5,9},{9,... | collective-permute-start | bytes 3080 | tf_op jit(solution)/shard_map/ppermute | solution.py:10
  164.9 3.3 %convolution_convert_fusion.1 = bf16[128,2048]{1,0:T(8,128)(2,1)} fusion(bf16[256,2048]{1,0:T(8,128)(2,1)} %param.20, bf16[2048,256]{1,0:T(8,128)(2,1)} %param.18, f32[130,256]{1,0:T(8,128)S(1)} %maximum_convert_fusion, f32[256]{0:T(256)S(1)} %bitcast.51, f32[256]{0:T(256)S(1)} %bitcast.52, f32[256]{0:T(256)S(1)} %bitcast.50, bf16[128,2048]{1,0:T(8,128)(2,1)} %param.14, ...), kind=kOutput, calls=%fused_computation.11 | convolution fusion | flops 269975552 | bytes 3550720 | tf_op jit(solution)/shard_map/dot_general | solution.py:49
  168.2 13.5 %all-to-all-done.1 = bf16[32,8,2048]{2,0,1:T(8,128)(2,1)S(1)} async-done(((bf16[32,8,2048]{2,0,1:T(8,128)(2,1)}), bf16[32,8,2048]{2,0,1:T(8,128)(2,1)S(1)}, u32[]{:S(2)}, u32[]{:S(2)}) %all-to-all-start.1) | async-done | bytes 1048608 | tf_op jit(solution)/shard_map/all_to_all | solution.py:88
  182.4 3.3 %gather_fusion.1 = bf16[512,2048]{1,0:T(8,128)(2,1)} fusion(bf16[257,2048]{1,0:T(8,128)(2,1)S(1)} %concatenate.11, s32[1024]{0:T(1024)S(1)} %pad_clamp_fusion), kind=kCustom, calls=%fused_computation.1 | custom fusion | bytes 4196352 | tf_op jit(solution)/shard_map/jit(_take)/gather | solution.py:108
  185.7 4.4 %gather.15 = bf16[256,2,2048]{2,1,0:T(2,128)(2,1)} reshape(bf16[512,2048]{1,0:T(8,128)(2,1)} %gather_fusion.1) | data formatting | bytes 4194304 | tf_op jit(solution)/shard_map/jit(_take)/gather | solution.py:108
  190.1 10.8 %multiply_reduce_fusion = bf16[256,2048]{1,0:T(8,128)(2,1)} fusion(bf16[256,2,2048]{2,1,0:T(2,128)(2,1)} %gather.15, pred[256,2]{1,0:T(8,128)(4,1)S(1)} %copy.74, f32[256,2]{1,0:T(8,128)S(1)} %copy.81), kind=kLoop, calls=%fused_computation.6 | loop fusion | flops 3670016 | bytes 3148288 | tf_op jit(solution)/shard_map/reduce_sum | solution.py:111
  201.0 43.5 %all-reduce.5.cloned.1.call-done = (bf16[128,2048]{1,0:T(8,128)(2,1)}, bf16[256,2048]{1,0:T(8,128)(2,1)}) async-done(((bf16[128,2048]{1,0:T(8,128)(2,1)}, bf16[256,2048]{1,0:T(8,128)(2,1)}), (bf16[128,2048]{1,0:T(8,128)(2,1)}, bf16[256,2048]{1,0:T(8,128)(2,1)})) %all-reduce.5.cloned.1.call-update) | async-done | bytes 1572880 | tf_op jit(solution)/shard_map/psum | solution.py:113
  244.5 1.9 copy.87
  246.4 2.3 copy.88
  (56 shorter events, 5.7 us)
Async XLA Ops:
  7.2 85.8 %copy-start = (bf16[1,512,2048]{2,1,0:T(8,128)(2,1)S(1)}, bf16[1,512,2048]{2,1,0:T(8,128)(2,1)}, u32[]{:S(2)}) copy-start(bf16[1,512,2048]{2,1,0:T(8,128)(2,1)} %param.27) | copy-start | bytes 6291460
  7.2 5.3 %copy-start.1 = (bf16[256,2048]{1,0:T(8,128)(2,1)S(1)}, bf16[256,2048]{1,0:T(8,128)(2,1)}, u32[]{:S(2)}) copy-start(bf16[256,2048]{1,0:T(8,128)(2,1)} %param.21) | copy-start | bytes 3145732
  7.2 79.2 %all-gather.2.cloned.1.call-start = ((), (), s32[]{:S(2)}) async-start(), calls=%async_computation.3 | async-start | bytes 5242880 | tf_op jit(solution)/shard_map/all_gather | solution.py:77
  52.8 95.0 %reduce-scatter.2.cloned.1.call-start = ((), (), s32[]{:S(2)}) async-start(), calls=%async_computation.4 | async-start | bytes 5242880 | tf_op jit(solution)/shard_map/reduce_scatter | solution.py:82
  103.0 1.0 copy-start.2
  147.7 8.4 %copy-start.3 = (f32[2048]{0:T(1024)S(1)}, f32[2048]{0:T(1024)}, u32[]{:S(2)}) copy-start(f32[2048]{0:T(1024)} %param.15) | copy-start | bytes 24580
  150.5 31.2 %all-to-all-start.1 = ((bf16[32,8,2048]{2,0,1:T(8,128)(2,1)}), bf16[32,8,2048]{2,0,1:T(8,128)(2,1)S(1)}, u32[]{:S(2)}, u32[]{:S(2)}) async-start(bf16[32,8,2048]{2,0,1:T(8,128)(2,1)} %copy.78), calls=%async_computation.2 | async-start | bytes 2097152 | tf_op jit(solution)/shard_map/all_to_all | solution.py:88
  156.0 8.1 %copy-start.4 = (s32[256,2]{0,1:T(2,128)S(1)}, s32[256,2]{0,1:T(2,128)}, u32[]{:S(2)}) copy-start(s32[256,2]{0,1:T(2,128)} %param.23) | copy-start | bytes 6148
  156.0 8.1 %copy-start.5 = (f32[3,256]{1,0:T(4,128)S(1)}, f32[3,256]{1,0:T(4,128)}, u32[]{:S(2)}) copy-start(f32[3,256]{1,0:T(4,128)} %param.19) | copy-start | bytes 9220
  156.0 88.4 %all-reduce.5.cloned.1.call-start = ((), (), s32[]{:S(2)}) async-start(), calls=%async_computation.5 | async-start | bytes 3145728 | tf_op jit(solution)/shard_map/psum | solution.py:113
  156.1 8.3 %copy-start.6 = (f32[256,2]{0,1:T(2,128)S(1)}, f32[256,2]{0,1:T(2,128)}, u32[]{:S(2)}) copy-start(f32[256,2]{0,1:T(2,128)} %param.24) | copy-start | bytes 6148
  159.7 5.2 %collective-permute-start = (bf16[2,256]{1,0:T(2,128)(2,1)S(1)}, bf16[2,256]{1,0:T(2,128)(2,1)S(1)}, u32[]{:S(2)}, u32[]{:S(2)}) collective-permute-start(bf16[2,256]{1,0:T(2,128)(2,1)S(1)} %slice.40), channel_id=1, source_target_pairs={{0,4},{4,8},{8,12},{12,16},{16,20},{20,24},{24,28},{1,5},{5,9},{9,... | collective-permute-start | bytes 3080 | tf_op jit(solution)/shard_map/ppermute | solution.py:10
Sparse Core Ops, SparseCore 0:
  52.9 33.4 all-gather.1
  103.1 44.5 reduce-scatter.1
  201.1 43.3 all-reduce.4
where the time goes:
time: 256 us; the launch traced here: 255 us
  waiting for transfers between devices  134 us (52%)
  blocking collectives  32.8 us (13%)
  matrix products  23.4 us (9%)
  local copies, waits for them, and re-layouts  22.8 us (9%)
  other arithmetic  18 us (7%)
  between operations  14 us (5%)
  starting transfers between devices  9.73 us (4%)
    reduce_scatter x1, waiting for transfers between devices, on_device(): lax.psum_scatter(jnp.dot(hidden, expert_down[0], preferred_element_type=j...  43.5 us
    psum x1, waiting for transfers between devices, on_device(): lax.psum(mixer_terms.astype(jnp.bfloat16), 'tp').astype(jnp.float32)  43.5 us
    all_gather x1, waiting for transfers between devices, on_device(): incoming = lax.all_gather(arrived, 'tp', axis=0, tiled=True)  33.6 us
    all_to_all x1, blocking collectives, on_device(): lax.all_to_all(outgoing, 'ep', split_axis=1, concat_axis=1, tiled=True)  32.8 us
    all_to_all x1, waiting for transfers between devices, on_device(): lax.all_to_all(summed.reshape(share_rows, experts, model_width), 'ep', sp...  13.5 us
    reduce_sum x1, other arithmetic, on_device(): jnp.sum(contrib.reshape(tok_count, pick_count, model_width), axis=1)  10.8 us
    dot_general x1, matrix products, on_device(): jnp.dot(hidden, expert_down[0], preferred_element_type=jnp.float32)  9.96 us
    gather x2, local copies, waits for them, and re-layouts, on_device(): jnp.take(flat_back, local_slot, axis=0).astype(jnp.float32)  7.75 us
  transfers between devices with their start and end apart: 5, of which 5 were waited for; matrix products, arithmetic and copies ran while one was open for 3% of the time, Pallas kernels for 0%

commit v1 on v0

--- a/solution.py
+++ b/solution.py
@@ -85,12 +85,18 @@
         scatter_dimension=0,
         tiled=True,
     )
-    returned = lax.all_to_all(
-        summed.reshape(share_rows, experts, model_width),
-        "ep",
-        split_axis=1,
-        concat_axis=1,
-        tiled=True,
+    returned = jnp.concatenate(
+        lax.all_to_all(
+            jnp.stack(
+                jnp.split(
+                    summed.reshape(share_rows, experts, model_width), lax.axis_size("ep"), axis=1
+                )
+            ),
+            "ep",
+            0,
+            0,
+        ),
+        axis=1,
     )
     flat_back = jnp.concatenate(
         [

time: 256 us -> 265 us (1.035)
  local copies, waits for them, and re-layouts: 22.8 us -> 32.4 us
    split x0 -> x1, local copies, waits for them, and re-layouts: none -> 6.5 us  [on_device(): jnp.split(summed.reshape(share_rows, experts, model_width), lax.axis_size...]
    unnamed x18 -> x25, local copies, waits for them, and re-layouts: 6.36 us -> 11.5 us
where the time goes in v1:
time: 265 us
  waiting for transfers between devices  135 us (51%)
  blocking collectives  32.8 us (12%)
  local copies, waits for them, and re-layouts  32.4 us (12%)
  matrix products  23.4 us (9%)
  other arithmetic  18 us (7%)
  between operations  14 us (5%)
  starting transfers between devices  9.55 us (4%)
    reduce_scatter x1, waiting for transfers between devices, on_device(): lax.psum_scatter(jnp.dot(hidden, expert_down[0], preferred_element_type=j...  43.5 us
    psum x1, waiting for transfers between devices, on_device(): lax.psum(mixer_terms.astype(jnp.bfloat16), 'tp').astype(jnp.float32)  43.5 us
    all_gather x1, waiting for transfers between devices, on_device(): incoming = lax.all_gather(arrived, 'tp', axis=0, tiled=True)  33.6 us
    all_to_all x1, blocking collectives, on_device(): lax.all_to_all(outgoing, 'ep', split_axis=1, concat_axis=1, tiled=True)  32.8 us
    all_to_all x1, waiting for transfers between devices, on_device(): lax.all_to_all(jnp.stack(jnp.split(summed.reshape(share_rows, experts, mo...  13.5 us
    unnamed x25, local copies, waits for them, and re-layouts  11.5 us
    reduce_sum x1, other arithmetic, on_device(): jnp.sum(contrib.reshape(tok_count, pick_count, model_width), axis=1)  10.8 us
    dot_general x1, matrix products, on_device(): jnp.dot(hidden, expert_down[0], preferred_element_type=jnp.float32)  9.96 us
  transfers between devices with their start and end apart: 5, of which 5 were waited for; matrix products, arithmetic and copies ran while one was open for 3% of the time, Pallas kernels for 0%

profile of v1, /device:TPU:0, one launch (start us, length us, event | category | flops | bytes accessed | tf_op | source)
XLA Modules:
  0.0 264.8 jit_solution(17510317270379526477)
XLA Ops:
  8.5 1.1 reduce-window.6
  10.9 1.5 fusion.4
  13.6 2.3 gather_fusion
  15.9 2.4 copy_select_fusion
  18.4 32.8 %all_to_all.10 = bf16[32,8,2048]{2,0,1:T(8,128)(2,1)S(1)} all-to-all(bf16[32,8,2048]{2,0,1:T(8,128)(2,1)S(1)} %copy_select_fusion), channel_id=1, replica_groups=mesh['ep'=8,'tp'=4] {'ep'}, dimensions={1} | all-to-all | bytes 2097152 | tf_op jit(solution)/shard_map/all_to_all | solution.py:76
  51.2 1.5 copy.108
  52.8 33.6 %all-gather.2.cloned.1.call-done = bf16[128,8,2048]{2,1,0:T(8,128)(2,1)} async-done(((bf16[32,8,2048]{2,1,0:T(8,128)(2,1)}), bf16[128,8,2048]{2,1,0:T(8,128)(2,1)}) %all-gather.2.cloned.1.call-update) | async-done | bytes 4194320 | tf_op jit(solution)/shard_map/all_gather | solution.py:77
  86.4 6.6 %fusion.2 = f32[1024,512]{1,0:T(8,128)} fusion(bf16[128,8,2048]{2,1,0:T(8,128)(2,1)} %all-gather.2.cloned.1.call-done, bf16[1,2048,512]{2,1,0:T(8,128)(2,1)} %param.25), kind=kOutput, calls=%fused_computation.4 | convolution fusion | flops 2147483648 | bytes 8388608 | tf_op jit(solution)/shard_map/dot_general | solution.py:79
  93.0 10.0 %convolution_convert_fusion = bf16[1024,2048]{1,0:T(8,128)(2,1)} fusion(bf16[1,512,2048]{2,1,0:T(8,128)(2,1)S(1)} %copy-done, f32[1024,512]{1,0:T(8,128)} %fusion.2, bf16[1,2048,512]{2,1,0:T(8,128)(2,1)} %param.26, bf16[128,8,2048]{2,1,0:T(8,128)(2,1)} %all-gather.2.cloned.1.call-done), kind=kOutput, calls=%fused_computation.8 | convolution fusion | flops 4300210176 | bytes 14680064 | tf_op jit(solution)/shard_map/dot_general | solution.py:83
  103.0 1.0 copy-done.2
  104.2 43.5 %reduce-scatter.2.cloned.1.call-done = bf16[256,2048]{1,0:T(8,128)(2,1)} async-done(((bf16[1024,2048]{1,0:T(8,128)(2,1)}), bf16[256,2048]{1,0:T(8,128)(2,1)}) %reduce-scatter.2.cloned.1.call-update) | async-done | bytes 1048592 | tf_op jit(solution)/shard_map/reduce_scatter | solution.py:82
  147.7 6.5 %fusion.52 = (bf16[32,1,2048]{2,1,0:T(2,128)(2,1)S(1)}, bf16[32,1,2048]{2,1,0:T(2,128)(2,1)S(1)}, bf16[32,1,2048]{2,1,0:T(2,128)(2,1)S(1)}, bf16[32,1,2048]{2,1,...) fusion(bf16[32,8,2048]{2,1,0:T(8,128)(2,1)} %bitcast.81), kind=kLoop, calls=%fused_computation.98 | loop fusion | bytes 2097152 | tf_op jit(solution)/shard_map/split | solution.py:91
  160.1 5.5 %all-to-all-start.1 = ((bf16[8,32,1,2048]{3,1,2,0:T(8,128)(2,1)}), bf16[8,32,1,2048]{3,1,2,0:T(8,128)(2,1)S(1)}, u32[]{:S(2)}, u32[]{:S(2)}) async-start(bf16[8,32,1,2048]{3,1,2,0:T(8,128)(2,1)} %fusion.29), calls=%async_computation.2 | async-start | bytes 2097152 | tf_op jit(solution)/shard_map/all_to_all | solution.py:89
  165.8 1.7 fusion.48
  167.5 1.7 fusion.16
  169.3 3.9 %collective-permute-start = (bf16[2,256]{1,0:T(2,128)(2,1)S(1)}, bf16[2,256]{1,0:T(2,128)(2,1)S(1)}, u32[]{:S(2)}, u32[]{:S(2)}) collective-permute-start(bf16[2,256]{1,0:T(2,128)(2,1)S(1)} %slice.40), channel_id=1, source_target_pairs={{0,4},{4,8},{8,12},{12,16},{16,20},{20,24},{24,28},{1,5},{5,9},{9,... | collective-permute-start | bytes 3080 | tf_op jit(solution)/shard_map/ppermute | solution.py:10
  174.5 3.3 %convolution_convert_fusion.1 = bf16[128,2048]{1,0:T(8,128)(2,1)} fusion(bf16[256,2048]{1,0:T(8,128)(2,1)} %param.20, bf16[2048,256]{1,0:T(8,128)(2,1)} %param.18, f32[130,256]{1,0:T(8,128)S(1)} %maximum_convert_fusion, f32[256]{0:T(256)S(1)} %bitcast.85, f32[256]{0:T(256)S(1)} %bitcast.86, f32[256]{0:T(256)S(1)} %bitcast.84, bf16[128,2048]{1,0:T(8,128)(2,1)} %param.14, ...), kind=kOutput, calls=%fused_computation.11 | convolution fusion | flops 269975552 | bytes 3550720 | tf_op jit(solution)/shard_map/dot_general | solution.py:49
  177.8 13.5 %all-to-all-done.1 = bf16[8,32,1,2048]{3,1,2,0:T(8,128)(2,1)S(1)} async-done(((bf16[8,32,1,2048]{3,1,2,0:T(8,128)(2,1)}), bf16[8,32,1,2048]{3,1,2,0:T(8,128)(2,1)S(1)}, u32[]{:S(2)}, u32[]{:S(2)}) %all-to-all-start.1) | async-done | bytes 1048608 | tf_op jit(solution)/shard_map/all_to_all | solution.py:89
  192.0 3.3 %gather_fusion.1 = bf16[512,2048]{1,0:T(8,128)(2,1)} fusion(bf16[257,2048]{1,0:T(8,128)(2,1)S(1)} %concatenate.11, s32[1024]{0:T(1024)S(1)} %pad_clamp_fusion), kind=kCustom, calls=%fused_computation.1 | custom fusion | bytes 4196352 | tf_op jit(solution)/shard_map/jit(_take)/gather | solution.py:114
  195.3 4.4 %gather.15 = bf16[256,2,2048]{2,1,0:T(2,128)(2,1)} reshape(bf16[512,2048]{1,0:T(8,128)(2,1)} %gather_fusion.1) | data formatting | bytes 4194304 | tf_op jit(solution)/shard_map/jit(_take)/gather | solution.py:114
  199.7 10.8 %multiply_reduce_fusion = bf16[256,2048]{1,0:T(8,128)(2,1)} fusion(bf16[256,2,2048]{2,1,0:T(2,128)(2,1)} %gather.15, pred[256,2]{1,0:T(8,128)(4,1)S(1)} %copy.105, f32[256,2]{1,0:T(8,128)S(1)} %copy.119), kind=kLoop, calls=%fused_computation.6 | loop fusion | flops 3670016 | bytes 3148288 | tf_op jit(solution)/shard_map/reduce_sum | solution.py:117
  210.6 43.5 %all-reduce.5.cloned.1.call-done = (bf16[128,2048]{1,0:T(8,128)(2,1)}, bf16[256,2048]{1,0:T(8,128)(2,1)}) async-done(((bf16[128,2048]{1,0:T(8,128)(2,1)}, bf16[256,2048]{1,0:T(8,128)(2,1)}), (bf16[128,2048]{1,0:T(8,128)(2,1)}, bf16[256,2048]{1,0:T(8,128)(2,1)})) %all-reduce.5.cloned.1.call-update) | async-done | bytes 1572880 | tf_op jit(solution)/shard_map/psum | solution.py:119
  254.1 1.9 copy.164
  256.0 2.3 copy.165
  (64 shorter events, 11.8 us)
Async XLA Ops:
  7.2 85.8 %copy-start = (bf16[1,512,2048]{2,1,0:T(8,128)(2,1)S(1)}, bf16[1,512,2048]{2,1,0:T(8,128)(2,1)}, u32[]{:S(2)}) copy-start(bf16[1,512,2048]{2,1,0:T(8,128)(2,1)} %param.27) | copy-start | bytes 6291460
  7.2 5.3 %copy-start.1 = (bf16[256,2048]{1,0:T(8,128)(2,1)S(1)}, bf16[256,2048]{1,0:T(8,128)(2,1)}, u32[]{:S(2)}) copy-start(bf16[256,2048]{1,0:T(8,128)(2,1)} %param.21) | copy-start | bytes 3145732
  7.2 79.2 %all-gather.2.cloned.1.call-start = ((), (), s32[]{:S(2)}) async-start(), calls=%async_computation.3 | async-start | bytes 5242880 | tf_op jit(solution)/shard_map/all_gather | solution.py:77
  52.8 95.0 %reduce-scatter.2.cloned.1.call-start = ((), (), s32[]{:S(2)}) async-start(), calls=%async_computation.4 | async-start | bytes 5242880 | tf_op jit(solution)/shard_map/reduce_scatter | solution.py:82
  103.0 1.0 copy-start.2
  156.4 9.3 %copy-start.3 = (f32[2048]{0:T(1024)S(1)}, f32[2048]{0:T(1024)}, u32[]{:S(2)}) copy-start(f32[2048]{0:T(1024)} %param.15) | copy-start | bytes 24580
  160.1 31.2 %all-to-all-start.1 = ((bf16[8,32,1,2048]{3,1,2,0:T(8,128)(2,1)}), bf16[8,32,1,2048]{3,1,2,0:T(8,128)(2,1)S(1)}, u32[]{:S(2)}, u32[]{:S(2)}) async-start(bf16[8,32,1,2048]{3,1,2,0:T(8,128)(2,1)} %fusion.29), calls=%async_computation.2 | async-start | bytes 2097152 | tf_op jit(solution)/shard_map/all_to_all | solution.py:89
  165.7 7.9 %copy-start.4 = (s32[256,2]{0,1:T(2,128)S(1)}, s32[256,2]{0,1:T(2,128)}, u32[]{:S(2)}) copy-start(s32[256,2]{0,1:T(2,128)} %param.23) | copy-start | bytes 6148
  165.7 8.0 %copy-start.5 = (f32[3,256]{1,0:T(4,128)S(1)}, f32[3,256]{1,0:T(4,128)}, u32[]{:S(2)}) copy-start(f32[3,256]{1,0:T(4,128)} %param.19) | copy-start | bytes 9220
  165.7 88.4 %all-reduce.5.cloned.1.call-start = ((), (), s32[]{:S(2)}) async-start(), calls=%async_computation.5 | async-start | bytes 3145728 | tf_op jit(solution)/shard_map/psum | solution.py:119
  165.7 8.1 %copy-start.6 = (f32[256,2]{0,1:T(2,128)S(1)}, f32[256,2]{0,1:T(2,128)}, u32[]{:S(2)}) copy-start(f32[256,2]{0,1:T(2,128)} %param.24) | copy-start | bytes 6148
  169.3 5.2 %collective-permute-start = (bf16[2,256]{1,0:T(2,128)(2,1)S(1)}, bf16[2,256]{1,0:T(2,128)(2,1)S(1)}, u32[]{:S(2)}, u32[]{:S(2)}) collective-permute-start(bf16[2,256]{1,0:T(2,128)(2,1)S(1)} %slice.40), channel_id=1, source_target_pairs={{0,4},{4,8},{8,12},{12,16},{16,20},{20,24},{24,28},{1,5},{5,9},{9,... | collective-permute-start | bytes 3080 | tf_op jit(solution)/shard_map/ppermute | solution.py:10
Sparse Core Ops, SparseCore 0:
  52.9 33.4 all-gather.1
  103.1 44.5 reduce-scatter.1
  210.7 43.3 all-reduce.4
